TPU v7x, 32 devices: a whole 2x2x4 slice. The times are simulated.
32 devices in a mesh: ep: 8 (over z, y), tp: 4 (over x, core).
Axes of the slice: x: 2, y: 2, z: 4, core: 2. Of those that a mesh axis runs over, the one named last changes fastest.
Arguments:
- query_rows: bfloat16 [3072, 1024], P('ep', 'tp'), may hold values from -6 to 6
- key_rows: bfloat16 [3072, 512], P('ep', 'tp'), may hold values from -6 to 6
- value_rows: bfloat16 [3072, 512], P('ep', 'tp'), may hold values from -6 to 6
- break_bias: bfloat16 [3072, 16], P('ep', 'tp'), may hold values from -14 to 0
- mixer_weight: bfloat16 [1024, 2048], P('tp'), may hold values from -0.1875 to 0.1875
- mixer_gain: bfloat16 [2048], replicated, may hold values from 0.099609375 to 1.8984375
- expert_input: bfloat16 [4096, 2048], P(('ep', 'tp')), may hold values from -6 to 6
- expert_gain: bfloat16 [2048], replicated, may hold values from 0.099609375 to 1.8984375
- route_ids: int32 [4096, 2], P('ep'), may hold values from 0 to 15, all different within a row; in each aligned block of 128 rows (0 to 127, 128 to 255, ...) at most 32 rows name the same one
- route_weights: float32 [4096, 2], P(('ep', 'tp')), may hold values from 0.2 to 2
- expert_gate: bfloat16 [16, 2048, 2048], P('ep', None, 'tp'), may hold values from -0.125 to 0.125
- expert_up: bfloat16 [16, 2048, 2048], P('ep', None, 'tp'), may hold values from -0.125 to 0.125
- expert_down: bfloat16 [16, 2048, 2048], P('ep', 'tp'), may hold values from -0.125 to 0.125
- shared_gate: bfloat16 [2048, 512], replicated, may hold values from -0.125 to 0.125
- shared_up: bfloat16 [2048, 512], replicated, may hold values from -0.125 to 0.125
- shared_down: bfloat16 [512, 2048], replicated, may hold values from -0.25 to 0.25
Outputs:
- mixer_out: bfloat16 [3072, 2048], P(('ep', 'tp'))
- expert_out: bfloat16 [4096, 2048], P(('ep', 'tp'))
Inputs may be any that keep to these rules, and one draw needn't show every extreme that they name: `route_ids`: each row names 2 different experts. Within the rows of one device no expert is named more than 32 times, and in every draw some expert is named exactly 32 times within the rows of some device.
All inputs are finite; a program needn't handle non-finite values.
Results may differ from a plain program's by a relative error of at most 0.012.
Values may be sent and summed in bfloat16 or wider, within the bound.
A program may use at most 192 MiB of HBM per device.

v0:
```python
import jax
import jax.numpy as jnp
from jax import lax
from jax.sharding import PartitionSpec as P

DH = 64
TOPK = 2
SEQS = 1
norm_eps = 1e-06


def rms_scale(values, gain):
    values = values.astype(jnp.float32)
    scale = lax.rsqrt(jnp.mean(values * values, axis=-1, keepdims=True) + norm_eps)
    return (values * scale * gain.astype(jnp.float32)).astype(jnp.bfloat16)


def break_terms(queries, key_block, bias_block, query_start, key_start):
    row_count = queries.shape[0]
    heads_local = queries.shape[1] * queries.shape[2]
    key_count = key_block.shape[0]
    scores = jnp.einsum("rkgd,skd->kgrs", queries, key_block, preferred_element_type=jnp.float32)
    scores = scores.reshape(heads_local, row_count, key_count) * DH ** (-0.5)
    scores = scores + bias_block.astype(jnp.float32).T[:, None, :]
    query_pos = query_start + jnp.arange(row_count, dtype=jnp.int32)
    key_pos = key_start + jnp.arange(key_count, dtype=jnp.int32)
    visible = key_pos[None, :] < query_pos[:, None]
    keep = jnp.where(visible, -jax.nn.softplus(scores), 0.0)
    beyond = lax.cumsum(keep, axis=2, reverse=True) - keep
    return (scores, visible, keep, beyond)


def block_values(scores, visible, beyond, value_block, groups):
    heads_local, row_count, key_count = scores.shape
    kv_local = value_block.shape[1]
    weights = jnp.where(visible, jnp.exp(jax.nn.log_sigmoid(scores) + beyond), 0.0).astype(
        jnp.bfloat16
    )
    weights = weights.reshape(kv_local, groups, row_count, key_count)
    summed = jnp.einsum("kgrs,skd->kgrd", weights, value_block, preferred_element_type=jnp.float32)
    return summed.reshape(heads_local, row_count, DH)


def on_device(
    query_rows,
    key_rows,
    value_rows,
    break_bias,
    mixer_weight,
    mixer_gain,
    expert_input,
    expert_gain,
    route_ids,
    route_weights,
    expert_gate,
    expert_up,
    expert_down,
    shared_gate,
    shared_up,
    shared_down,
):
    row_count = query_rows.shape[0]
    heads_local = query_rows.shape[1] // DH
    kv_local = key_rows.shape[1] // DH
    groups = heads_local // kv_local
    queries = query_rows.reshape(row_count, kv_local, groups, DH)
    ep_size = lax.axis_size("ep")
    device = lax.axis_index("ep")
    query_start = device * row_count
    span_shards = ep_size // SEQS

    def wanted(shard):
        return (shard <= device) & (shard // span_shards == device // span_shards)

    def shard_slice(piece, index):
        return lax.dynamic_slice_in_dim(piece, index * row_count, row_count, 0)

    empty_totals = jnp.zeros((ep_size, heads_local, row_count), jnp.float32)
    empty_output = jnp.zeros((heads_local, row_count, DH), jnp.float32)
    empty_parts = jnp.zeros((ep_size, heads_local, row_count, DH), jnp.float32)
    key_piece = lax.all_gather(key_rows, "ep", axis=0, tiled=True)
    value_piece = lax.all_gather(value_rows, "ep", axis=0, tiled=True)
    bias_piece = lax.all_gather(break_bias, "ep", axis=0, tiled=True)

    def one_shard(index, current):
        parts, totals = current
        shard = index
        key_block = shard_slice(key_piece, index).reshape(row_count, kv_local, DH)
        value_block = shard_slice(value_piece, index).reshape(row_count, kv_local, DH)
        bias_block = shard_slice(bias_piece, index)

        def compute(unused):
            scores, visible, keep, beyond = break_terms(
                queries, key_block, bias_block, query_start, shard * row_count
            )
            return (
                block_values(scores, visible, beyond, value_block, groups),
                jnp.sum(keep, axis=2),
            )

        def skipped(unused):
            return (empty_output, jnp.zeros((heads_local, row_count), jnp.float32))

        block_part, total = lax.cond(wanted(shard), compute, skipped, None)
        parts = lax.dynamic_update_index_in_dim(parts, block_part, shard, 0)
        totals = lax.dynamic_update_index_in_dim(totals, total, shard, 0)
        return (parts, totals)

    parts, totals = lax.fori_loop(
        0, key_piece.shape[0] // row_count, one_shard, (empty_parts, empty_totals)
    )
    later = jnp.sum(totals, axis=0) - jnp.cumsum(totals, axis=0)
    output = jnp.sum(jnp.exp(later)[..., None] * parts, axis=0)
    attended = output.transpose(1, 0, 2).reshape(row_count, heads_local * DH).astype(jnp.bfloat16)
    block = attended
    projected = lax.psum_scatter(
        jnp.dot(block, mixer_weight, preferred_element_type=jnp.float32).astype(jnp.bfloat16),
        "tp",
        scatter_dimension=0,
        tiled=True,
    ).astype(jnp.float32)
    mixer_out = rms_scale(projected, mixer_gain)
    token_count = expert_input.shape[0]
    width = expert_input.shape[1]
    local_experts = expert_gate.shape[0]
    experts_all = local_experts * ep_size
    capacity = 2 * token_count * TOPK // experts_all
    tp_index = lax.axis_index("tp")
    normed = rms_scale(expert_input, expert_gain)
    flat = lax.dynamic_slice_in_dim(route_ids, tp_index * token_count, token_count, 0).reshape(-1)
    onehot = (flat[:, None] == jnp.arange(experts_all, dtype=jnp.int32)[None, :]).astype(jnp.int32)
    before = jnp.cumsum(onehot, axis=0) - onehot
    own_slots = flat * capacity + jnp.sum(before * onehot, axis=1)
    owners = jnp.full((experts_all * capacity,), token_count, jnp.int32)
    owners = owners.at[own_slots].set(jnp.arange(own_slots.shape[0], dtype=jnp.int32) // TOPK)
    padded = jnp.concatenate([normed, jnp.zeros((1, width), normed.dtype)], axis=0)
    outgoing = padded[owners].reshape(ep_size, local_experts, capacity, width)[None]
    arrived = lax.all_to_all(outgoing, "ep", split_axis=1, concat_axis=1, tiled=True)
    piece = lax.all_gather(arrived, "tp", axis=0, tiled=True)
    gate_proj = jnp.einsum(
        "pnecd,edf->pnecf", piece, expert_gate, preferred_element_type=jnp.float32
    )
    up_proj = jnp.einsum("pnecd,edf->pnecf", piece, expert_up, preferred_element_type=jnp.float32)
    hidden = (jax.nn.silu(gate_proj) * up_proj).astype(jnp.bfloat16)
    block = hidden
    summed = lax.psum_scatter(
        jnp.einsum(
            "pnecf,efd->pnecd", block, expert_down, preferred_element_type=jnp.float32
        ).astype(jnp.bfloat16),
        "tp",
        scatter_dimension=0,
        tiled=True,
    )
    returned = lax.all_to_all(
        summed.reshape(ep_size, local_experts * capacity, width),
        "ep",
        split_axis=0,
        concat_axis=0,
        tiled=True,
    )
    results = returned.reshape(experts_all * capacity, width)
    picked = results[own_slots].reshape(token_count, TOPK, width).astype(jnp.float32)
    routed = jnp.einsum("tk,tkd->td", route_weights, picked)
    shared_hidden = (
        jax.nn.silu(jnp.dot(normed, shared_gate, preferred_element_type=jnp.float32))
        * jnp.dot(normed, shared_up, preferred_element_type=jnp.float32)
    ).astype(jnp.bfloat16)
    expert_out = (
        routed + jnp.dot(shared_hidden, shared_down, preferred_element_type=jnp.float32)
    ).astype(jnp.bfloat16)
    return (mixer_out, expert_out)


def solution(mesh):
    return jax.shard_map(
        on_device,
        mesh=mesh,
        in_specs=(
            P("ep", "tp"),
            P("ep", "tp"),
            P("ep", "tp"),
            P("ep", "tp"),
            P("tp", None),
            P(),
            P(("ep", "tp"), None),
            P(),
            P("ep", None),
            P(("ep", "tp"), None),
            P("ep", None, "tp"),
            P("ep", None, "tp"),
            P("ep", "tp", None),
            P(),
            P(),
            P(),
        ),
        out_specs=(P(("ep", "tp"), None), P(("ep", "tp"), None)),
        check_vma=False,
    )
```

profile of v0, /device:TPU:0, one launch (start us, length us, event | category | flops | bytes accessed | tf_op | source)
XLA Modules:
  0.0 609.5 jit_solution(3167960819655452069)
XLA Ops:
  9.7 1.4 scatter_custom_fusion
  14.3 3.3 gather_fusion
  17.7 55.5 %all_to_all.10 = bf16[1,8,2,32,2048]{4,3,0,2,1:T(8,128)(2,1)S(1)} all-to-all(bf16[1,8,2,32,2048]{4,3,0,2,1:T(8,128)(2,1)} %bitcast.134), channel_id=1, replica_groups=mesh['ep'=8,'tp'=4] {'ep'}, dimensions={1} | all-to-all | bytes 4194304 | tf_op jit(solution)/shard_map/all_to_all | solution.py:138
  73.2 1.5 copy.50
  74.8 57.4 %all-gather.2.cloned.1.call-done = bf16[4,8,2,32,2048]{4,3,1,0,2:T(8,128)(2,1)} async-done(((bf16[1,8,2,32,2048]{4,3,1,0,2:T(8,128)(2,1)}), bf16[4,8,2,32,2048]{4,3,1,0,2:T(8,128)(2,1)}) %all-gather.2.cloned.1.call-update) | async-done | bytes 8388624 | tf_op jit(solution)/shard_map/all_gather | solution.py:139
  132.1 11.0 %fusion.26 = f32[2,4,8,32,512]{4,3,2,1,0:T(8,128)} fusion(bf16[4,8,2,32,2048]{4,3,1,0,2:T(8,128)(2,1)} %all-gather.2.cloned.1.call-done, bf16[2,2048,512]{2,1,0:T(8,128)(2,1)} %param.31), kind=kOutput, calls=%fused_computation.47 | convolution fusion | flops 4294967296 | bytes 16777216 | tf_op jit(solution)/shard_map/pnecd,edf->pnecf/dot_general | solution.py:143
  143.1 15.4 %convert_bitcast_fusion.2 = bf16[4,8,2,32,2048]{4,3,1,0,2:T(8,128)(2,1)} fusion(bf16[2,512,2048]{2,1,0:T(8,128)(2,1)} %param.32, f32[2,4,8,32,512]{4,3,2,1,0:T(8,128)} %fusion.26, bf16[4,8,2,32,2048]{4,3,1,0,2:T(8,128)(2,1)} %all-gather.2.cloned.1.call-done, bf16[2,2048,512]{2,1,0:T(8,128)(2,1)} %param.30), kind=kOutput, calls=%fused_computation.45 | convolution fusion | flops 8600420352 | bytes 29360128 | tf_op jit(solution)/shard_map/pnecf,efd->pnecd/dot_general | solution.py:147
  159.9 32.1 %all_gather.13 = bf16[3072,4]{0,1:T(4,128)(2,1)} all-gather(bf16[384,4]{0,1:T(4,128)(2,1)S(1)} %copy-done.8), channel_id=1, replica_groups=mesh['ep'=8,'tp'=4] {'ep'}, dimensions={0}, use_global_device_ids=true | all-gather | bytes 27648 | tf_op jit(solution)/shard_map/all_gather | solution.py:83
  192.0 34.8 %all_gather.12 = bf16[3072,128]{0,1:T(8,128)(2,1)} all-gather(bf16[384,128]{0,1:T(8,128)(2,1)S(1)} %copy.42), channel_id=1, replica_groups=mesh['ep'=8,'tp'=4] {'ep'}, dimensions={0}, use_global_device_ids=true | all-gather | bytes 884736 | tf_op jit(solution)/shard_map/all_gather | solution.py:81
  226.8 34.0 %all_gather.14 = bf16[3072,128]{0,1:T(8,128)(2,1)} all-gather(bf16[384,128]{0,1:T(8,128)(2,1)S(1)} %copy.44), channel_id=1, replica_groups=mesh['ep'=8,'tp'=4] {'ep'}, dimensions={0}, use_global_device_ids=true | all-gather | bytes 884736 | tf_op jit(solution)/shard_map/all_gather | solution.py:82
  260.9 41.2 %while.18 = (s32[]{:T(128)}, f32[8,4,384,64]{2,3,1,0:T(8,128)}, f32[8,4,384]{2,1,0:T(4,128)S(1)}, s32[]{:T(128)}, s32[]{:T(128)}, /*index=5*/s32[]{:T(128)}, bf1...) while((s32[]{:T(128)}, f32[8,4,384,64]{2,3,1,0:T(8,128)}, ...), condition=%wide.region_6.7_spmd, body=%wide.region_0.6_spmd.sunk | while | flops 250984336 | bytes 43047352 | solution.py:109
  260.9 34.5 %conditional.2 = (f32[1,4,384,64]{2,3,1,0:T(8,128)S(1)}, f32[1,4,384]{2,1,0:T(4,128)S(1)}) conditional(s32[]{:T(128)} %convert_element_type.126, () %tuple.76, (s32[]{:T(128)}, s32[]{:T(128)}, bf16[3072,128]{0,1:T(8,128)(2,1)}, bf16[384,2,2,64]{0,3,2,1:T(8,128)(2,1)S(1)}, bf16[3072,4]{0,1:T(4,128)(2,1)}, /*index=5*/bf16[3072,128]{0,1:T(8,128)(2,1)}) %tuple.77), branch_computations={%region_1.1_spmd, %region_2.5_spmd} | conditional | flops 250984320 | bytes 42247824 | solution.py:104
  262.7 3.4 fusion.17
  266.5 19.3 %fusion.2 = f32[4,384,3,128]{1,2,3,0:T(4,128)S(1)} fusion(f32[4,384,3,128]{1,3,2,0:T(8,128)} %bitcast.131, f32[4,3,128]{1,2,0:T(8,128)S(1)} %copy.38, pred[384,3,128]{0,1,2:T(4,128)(4,1)S(1)} %broadcast_compare_fusion), kind=kOutput, calls=%fused_computation.8 | output fusion | flops 80216064 | bytes 4872192 | tf_op jit(solution)/shard_map/reduce-window.10
  285.8 1.7 copy-done.1
  287.6 2.5 broadcast_add_fusion
  290.3 1.4 copy-done.2
  291.8 3.6 fusion.21
  302.1 2.3 multiply_reduce_fusion
  304.4 1.8 convolution_convert_fusion
  306.8 4.8 all-reduce.4.cloned.1.call-done
  311.6 2.4 constant_dynamic-slice_fusion.2
  313.9 1.4 copy.51
  315.4 241.3 %all-to-all-start.1 = ((bf16[8,64,2048]{2,1,0:T(8,128)(2,1)}), bf16[8,64,2048]{2,1,0:T(8,128)(2,1)}, u32[]{:S(2)}, u32[]{:S(2)}) async-start(bf16[8,64,2048]{2,1,0:T(8,128)(2,1)} %bitcast.135), calls=%async_computation.2 | async-start | bytes 4194304 | tf_op jit(solution)/shard_map/all_to_all | solution.py:154
  556.8 2.0 fusion.62
  558.9 15.9 %reduce-scatter.5.cloned.1.call-done = bf16[96,2048]{1,0:T(8,128)(2,1)} async-done(((bf16[384,2048]{1,0:T(8,128)(2,1)}), bf16[96,2048]{1,0:T(8,128)(2,1)}) %reduce-scatter.5.cloned.1.call-update) | async-done | bytes 393232 | tf_op jit(solution)/shard_map/reduce_scatter | solution.py:116
  576.0 1.9 fusion.46
  577.9 10.2 %all-to-all-done.1 = bf16[8,64,2048]{2,1,0:T(8,128)(2,1)} async-done(((bf16[8,64,2048]{2,1,0:T(8,128)(2,1)}), bf16[8,64,2048]{2,1,0:T(8,128)(2,1)}, u32[]{:S(2)}, u32[]{:S(2)}) %all-to-all-start.1) | async-done | bytes 2097184 | tf_op jit(solution)/shard_map/all_to_all | solution.py:154
  588.0 5.2 gather_fusion.1
  593.2 2.5 reshape.199
  595.8 3.5 fusion.61
  599.3 3.7 fusion.36
  (110 shorter events, 18.4 us)
Async XLA Ops:
  7.2 592.1 %copy-start = (bf16[512,2048]{1,0:T(8,128)(2,1)S(1)}, bf16[512,2048]{1,0:T(8,128)(2,1)}, u32[]{:S(2)}) copy-start(bf16[512,2048]{1,0:T(8,128)(2,1)} %param.35) | copy-start | bytes 6291460
  7.2 124.9 %all-gather.2.cloned.1.call-start = ((), (), s32[]{:S(2)}) async-start(), calls=%async_computation.4 | async-start | bytes 10485760 | tf_op jit(solution)/shard_map/all_gather | solution.py:139
  74.7 236.9 %all-reduce.4.cloned.1.call-start = ((), (), s32[]{:S(2)}) async-start(), calls=%async_computation.5 | async-start | bytes 16777216
  158.5 0.9 copy-start.5
  158.5 1.0 copy-start.6
  158.5 1.2 copy-start.4
  158.5 1.3 copy-start.8
  158.6 416.2 %reduce-scatter.5.cloned.1.call-start = ((), (), s32[]{:S(2)}) async-start(), calls=%async_computation.3 | async-start | bytes 1966080 | tf_op jit(solution)/shard_map/reduce_scatter | solution.py:116
  285.8 1.7 copy-start.1
  290.1 1.7 copy-start.2
  302.1 2.3 copy-start.3
  304.4 1.8 copy-start.10
  315.4 241.3 %copy-start.9 = (f32[128,2]{0,1:T(2,128)S(1)}, f32[128,2]{0,1:T(2,128)}, u32[]{:S(2)}) copy-start(f32[128,2]{0,1:T(2,128)} %param.29) | copy-start | bytes 3076
  315.4 241.4 %copy-start.7 = (bf16[2048]{0:T(1024)(128)(2,1)S(1)}, bf16[2048]{0:T(1024)(128)(2,1)}, u32[]{:S(2)}) copy-start(bf16[2048]{0:T(1024)(128)(2,1)} %param.25) | copy-start | bytes 12292
  315.4 272.7 %all-to-all-start.1 = ((bf16[8,64,2048]{2,1,0:T(8,128)(2,1)}), bf16[8,64,2048]{2,1,0:T(8,128)(2,1)}, u32[]{:S(2)}, u32[]{:S(2)}) async-start(bf16[8,64,2048]{2,1,0:T(8,128)(2,1)} %bitcast.135), calls=%async_computation.2 | async-start | bytes 4194304 | tf_op jit(solution)/shard_map/all_to_all | solution.py:154
Sparse Core Ops, SparseCore 0:
  74.8 57.2 all-gather.1
  158.7 152.8 all-reduce.3
  314.1 260.6 reduce-scatter.4
where the time goes:
time: 611 us; the launch traced here: 609 us
  starting transfers between devices  241 us (39%)
  blocking collectives  157 us (26%)
  waiting for transfers between devices  88.2 us (14%)
  matrix products  44.3 us (7%)
  other arithmetic  33 us (5%)
  local copies, waits for them, and re-layouts  31.7 us (5%)
  between operations  14 us (2%)
    all_to_all x1, starting transfers between devices, on_device(): lax.all_to_all(summed.reshape(ep_size, local_experts * capacity, width),...  241 us
    all_gather x1, waiting for transfers between devices, on_device(): piece = lax.all_gather(arrived, 'tp', axis=0, tiled=True)  57.4 us
    all_to_all x1, blocking collectives, on_device(): lax.all_to_all(outgoing, 'ep', split_axis=1, concat_axis=1, tiled=True)  55.5 us
    all_gather x1, blocking collectives, on_device(): key_piece = lax.all_gather(key_rows, 'ep', axis=0, tiled=True)  34.8 us
    all_gather x1, blocking collectives, on_device(): value_piece = lax.all_gather(value_rows, 'ep', axis=0, tiled=True)  34 us
    all_gather x1, blocking collectives, on_device(): bias_piece = lax.all_gather(break_bias, 'ep', axis=0, tiled=True)  32.1 us
    another operation x4, other arithmetic  20 us
    reduce_scatter x1, waiting for transfers between devices, on_device(): lax.psum_scatter(jnp.dot(block, mixer_weight, preferred_element_type=jnp....  15.9 us
  transfers between devices with their start and end apart: 4, of which 4 were waited for; matrix products, arithmetic and copies ran while one was open for 9% of the time, Pallas kernels for 0%

commit v1 on v0

--- a/solution.py
+++ b/solution.py
@@ -78,8 +78,9 @@
     empty_totals = jnp.zeros((ep_size, heads_local, row_count), jnp.float32)
     empty_output = jnp.zeros((heads_local, row_count, DH), jnp.float32)
     empty_parts = jnp.zeros((ep_size, heads_local, row_count, DH), jnp.float32)
-    key_piece = lax.all_gather(key_rows, "ep", axis=0, tiled=True)
-    value_piece = lax.all_gather(value_rows, "ep", axis=0, tiled=True)
+    extra = jnp.concatenate([key_rows, value_rows], axis=1)
+    y2 = lax.all_gather(extra, axis_name="ep", axis=0, tiled=True)
+    key_piece, value_piece = jnp.split(y2, [key_rows.shape[1]], axis=1)
     bias_piece = lax.all_gather(break_bias, "ep", axis=0, tiled=True)
 
     def one_shard(index, current):

time: 611 us -> 557 us (0.912)
  waiting for transfers between devices: 88.2 us -> 186 us
  starting transfers between devices: 241 us -> 154 us
  blocking collectives: 157 us -> 87.9 us
    all_to_all x1, starting transfers between devices: 241 us -> 154 us  [on_device(): lax.all_to_all(summed.reshape(ep_size, local_experts * capacity, width),...]
    unnamed x4 -> x5, waiting for transfers between devices: 4.81 us -> 92.1 us
    all_gather x2 -> x0, blocking collectives: 68.9 us -> none  [the longest x1 34.8 us: on_device(): key_piece = lax.all_gather(key_rows, 'ep', axis=0, tiled=True)]
    all_to_all x1, waiting for transfers between devices: 10.2 us -> 21.5 us  [on_device(): lax.all_to_all(summed.reshape(ep_size, local_experts * capacity, width),...]
  transfers between devices with their start and end apart: 4 -> 5, of which waited for: 4 -> 4; matrix products, arithmetic and copies ran while one was open for 9% -> 15% of each run, Pallas kernels for 0% -> 0%
where the time goes in v1:
time: 557 us; the launch traced here: 555 us
  waiting for transfers between devices  186 us (33%)
  starting transfers between devices  154 us (28%)
  blocking collectives  87.9 us (16%)
  matrix products  44.3 us (8%)
  local copies, waits for them, and re-layouts  34.4 us (6%)
  other arithmetic  34 us (6%)
  between operations  14 us (3%)
    all_to_all x1, starting transfers between devices, on_device(): lax.all_to_all(summed.reshape(ep_size, local_experts * capacity, width),...  154 us
    unnamed x5, waiting for transfers between devices  92.1 us
    all_gather x1, waiting for transfers between devices, on_device(): piece = lax.all_gather(arrived, 'tp', axis=0, tiled=True)  56.3 us
    all_to_all x1, blocking collectives, on_device(): lax.all_to_all(outgoing, 'ep', split_axis=1, concat_axis=1, tiled=True)  55.5 us
    all_gather x1, blocking collectives, on_device(): bias_piece = lax.all_gather(break_bias, 'ep', axis=0, tiled=True)  32.4 us
    all_to_all x1, waiting for transfers between devices, on_device(): lax.all_to_all(summed.reshape(ep_size, local_experts * capacity, width),...  21.5 us
    another operation x4, other arithmetic  20 us
    reduce_scatter x1, waiting for transfers between devices, on_device(): lax.psum_scatter(jnp.dot(block, mixer_weight, preferred_element_type=jnp....  16.2 us
  transfers between devices with their start and end apart: 5, of which 4 were waited for; matrix products, arithmetic and copies ran while one was open for 15% of the time, Pallas kernels for 0%

profile of v1, /device:TPU:0, one launch (start us, length us, event | category | flops | bytes accessed | tf_op | source)
XLA Modules:
  0.0 555.2 jit_solution(3536465360401230055)
XLA Ops:
  9.7 1.4 scatter_custom_fusion
  13.0 1.2 fusion.43
  14.3 3.3 gather_fusion
  17.7 55.5 %all_to_all.10 = bf16[1,8,2,32,2048]{4,3,0,2,1:T(8,128)(2,1)S(1)} all-to-all(bf16[1,8,2,32,2048]{4,3,0,2,1:T(8,128)(2,1)} %bitcast.134), channel_id=1, replica_groups=mesh['ep'=8,'tp'=4] {'ep'}, dimensions={1} | all-to-all | bytes 4194304 | tf_op jit(solution)/shard_map/all_to_all | solution.py:139
  73.2 1.5 copy.50
  75.8 56.3 %all-gather.5.cloned.1.call-done = bf16[4,8,2,32,2048]{4,3,1,0,2:T(8,128)(2,1)} async-done(((bf16[1,8,2,32,2048]{4,3,1,0,2:T(8,128)(2,1)}), bf16[4,8,2,32,2048]{4,3,1,0,2:T(8,128)(2,1)}) %all-gather.5.cloned.1.call-update) | async-done | bytes 8388624 | tf_op jit(solution)/shard_map/all_gather | solution.py:140
  132.1 11.0 %fusion.26 = f32[2,4,8,32,512]{4,3,2,1,0:T(8,128)} fusion(bf16[4,8,2,32,2048]{4,3,1,0,2:T(8,128)(2,1)} %all-gather.5.cloned.1.call-done, bf16[2,2048,512]{2,1,0:T(8,128)(2,1)} %param.31), kind=kOutput, calls=%fused_computation.47 | convolution fusion | flops 4294967296 | bytes 16777216 | tf_op jit(solution)/shard_map/pnecd,edf->pnecf/dot_general | solution.py:144
  143.1 15.4 %convert_bitcast_fusion.2 = bf16[4,8,2,32,2048]{4,3,1,0,2:T(8,128)(2,1)} fusion(bf16[2,512,2048]{2,1,0:T(8,128)(2,1)} %param.32, f32[2,4,8,32,512]{4,3,2,1,0:T(8,128)} %fusion.26, bf16[4,8,2,32,2048]{4,3,1,0,2:T(8,128)(2,1)} %all-gather.5.cloned.1.call-done, bf16[2,2048,512]{2,1,0:T(8,128)(2,1)} %param.30), kind=kOutput, calls=%fused_computation.45 | convolution fusion | flops 8600420352 | bytes 29360128 | tf_op jit(solution)/shard_map/pnecf,efd->pnecd/dot_general | solution.py:148
  159.6 32.4 %all_gather.10 = bf16[3072,4]{0,1:T(4,128)(2,1)} all-gather(bf16[384,4]{0,1:T(4,128)(2,1)S(1)} %copy-done.8), channel_id=1, replica_groups=mesh['ep'=8,'tp'=4] {'ep'}, dimensions={0}, use_global_device_ids=true | all-gather | bytes 27648 | tf_op jit(solution)/shard_map/all_gather | solution.py:84
  192.0 2.7 fusion.61
  194.7 41.4 %while.18 = (s32[]{:T(128)}, f32[8,4,384,64]{2,3,1,0:T(8,128)}, f32[8,4,384]{2,1,0:T(4,128)S(1)}, s32[]{:T(128)}, s32[]{:T(128)}, /*index=5*/s32[]{:T(128)}, bf1...) while((s32[]{:T(128)}, f32[8,4,384,64]{2,3,1,0:T(8,128)}, ...), condition=%wide.region_6.7_spmd, body=%wide.region_0.6_spmd.sunk | while | flops 250984336 | bytes 43047352 | solution.py:110
  194.7 34.7 %conditional.2 = (f32[1,4,384,64]{2,3,1,0:T(8,128)S(1)}, f32[1,4,384]{2,1,0:T(4,128)S(1)}) conditional(s32[]{:T(128)} %convert_element_type.126, () %tuple.77, (s32[]{:T(128)}, s32[]{:T(128)}, bf16[3072,128]{0,1:T(8,128)(2,1)}, bf16[384,2,2,64]{0,3,2,1:T(8,128)(2,1)S(1)}, bf16[3072,4]{0,1:T(4,128)(2,1)}, /*index=5*/bf16[3072,128]{0,1:T(8,128)(2,1)}) %tuple.78), branch_computations={%region_1.1_spmd, %region_2.5_spmd} | conditional | flops 250984320 | bytes 42247824 | solution.py:105
  196.5 3.4 fusion.17
  200.4 19.3 %fusion.2 = f32[4,384,3,128]{1,2,3,0:T(4,128)S(1)} fusion(f32[4,384,3,128]{1,3,2,0:T(8,128)} %bitcast.131, f32[4,3,128]{1,2,0:T(8,128)S(1)} %copy.38, pred[384,3,128]{0,1,2:T(4,128)(4,1)S(1)} %broadcast_compare_fusion), kind=kOutput, calls=%fused_computation.8 | output fusion | flops 80216064 | bytes 4872192 | tf_op jit(solution)/shard_map/reduce-window.10
  219.7 1.7 copy-done.1
  221.4 2.7 broadcast_add_fusion
  224.4 1.4 copy-done.2
  225.8 3.6 fusion.21
  236.2 2.3 multiply_reduce_fusion
  238.5 1.8 convolution_convert_fusion
  240.9 92.1 %all-reduce.4.cloned.1.call-done = bf16[4,8,2,32,2048]{4,3,1,0,2:T(8,128)(2,1)} async-done(((bf16[4,8,2,32,2048]{4,3,1,0,2:T(8,128)(2,1)}), bf16[4,8,2,32,2048]{4,3,1,0,2:T(8,128)(2,1)}) %all-reduce.4.cloned.1.call-update) | async-done | bytes 8388624
  333.0 2.4 constant_dynamic-slice_fusion.2
  335.4 1.4 copy.51
  336.8 153.9 %all-to-all-start.1 = ((bf16[8,64,2048]{2,1,0:T(8,128)(2,1)}), bf16[8,64,2048]{2,1,0:T(8,128)(2,1)}, u32[]{:S(2)}, u32[]{:S(2)}) async-start(bf16[8,64,2048]{2,1,0:T(8,128)(2,1)} %bitcast.135), calls=%async_computation.2 | async-start | bytes 4194304 | tf_op jit(solution)/shard_map/all_to_all | solution.py:155
  490.9 2.0 fusion.63
  493.0 16.2 %reduce-scatter.5.cloned.1.call-done = bf16[96,2048]{1,0:T(8,128)(2,1)} async-done(((bf16[384,2048]{1,0:T(8,128)(2,1)}), bf16[96,2048]{1,0:T(8,128)(2,1)}) %reduce-scatter.5.cloned.1.call-update) | async-done | bytes 393232 | tf_op jit(solution)/shard_map/reduce_scatter | solution.py:117
  510.3 1.9 fusion.46
  512.3 21.5 %all-to-all-done.1 = bf16[8,64,2048]{2,1,0:T(8,128)(2,1)} async-done(((bf16[8,64,2048]{2,1,0:T(8,128)(2,1)}), bf16[8,64,2048]{2,1,0:T(8,128)(2,1)}, u32[]{:S(2)}, u32[]{:S(2)}) %all-to-all-start.1) | async-done | bytes 2097184 | tf_op jit(solution)/shard_map/all_to_all | solution.py:155
  533.8 5.2 gather_fusion.1
  539.0 2.5 reshape.199
  541.5 3.5 fusion.62
  545.0 3.7 fusion.36
  (113 shorter events, 17.9 us)
Async XLA Ops:
  7.2 537.8 %copy-start = (bf16[512,2048]{1,0:T(8,128)(2,1)S(1)}, bf16[512,2048]{1,0:T(8,128)(2,1)}, u32[]{:S(2)}) copy-start(bf16[512,2048]{1,0:T(8,128)(2,1)} %param.35) | copy-start | bytes 6291460
  7.2 125.0 %all-gather.5.cloned.1.call-start = ((), (), s32[]{:S(2)}) async-start(), calls=%async_computation.5 | async-start | bytes 10485760 | tf_op jit(solution)/shard_map/all_gather | solution.py:140
  73.2 1.6 copy-start.5
  73.2 1.7 copy-start.6
  74.7 117.3 %all-gather.3.cloned.1.call-start = ((), (), s32[]{:S(2)}) async-start(), calls=%async_computation.3 | async-start | bytes 1769472 | tf_op jit(solution)/shard_map/all_gather | solution.py:82
  75.8 257.2 %all-reduce.4.cloned.1.call-start = ((), (), s32[]{:S(2)}) async-start(), calls=%async_computation.6 | async-start | bytes 16777216
  158.5 0.9 copy-start.4
  158.5 1.1 copy-start.8
  158.5 350.6 %reduce-scatter.5.cloned.1.call-start = ((), (), s32[]{:S(2)}) async-start(), calls=%async_computation.4 | async-start | bytes 1966080 | tf_op jit(solution)/shard_map/reduce_scatter | solution.py:117
  219.7 1.7 copy-start.1
  224.1 1.7 copy-start.2
  236.1 2.4 copy-start.3
  238.5 1.8 copy-start.10
  336.8 153.9 %copy-start.9 = (f32[128,2]{0,1:T(2,128)S(1)}, f32[128,2]{0,1:T(2,128)}, u32[]{:S(2)}) copy-start(f32[128,2]{0,1:T(2,128)} %param.29) | copy-start | bytes 3076
  336.8 154.1 %copy-start.7 = (bf16[2048]{0:T(1024)(128)(2,1)S(1)}, bf16[2048]{0:T(1024)(128)(2,1)}, u32[]{:S(2)}) copy-start(bf16[2048]{0:T(1024)(128)(2,1)} %param.25) | copy-start | bytes 12292
  336.8 196.9 %all-to-all-start.1 = ((bf16[8,64,2048]{2,1,0:T(8,128)(2,1)}), bf16[8,64,2048]{2,1,0:T(8,128)(2,1)}, u32[]{:S(2)}, u32[]{:S(2)}) async-start(bf16[8,64,2048]{2,1,0:T(8,128)(2,1)} %bitcast.135), calls=%async_computation.2 | async-start | bytes 4194304 | tf_op jit(solution)/shard_map/all_to_all | solution.py:155
Sparse Core Ops, SparseCore 0:
  74.8 57.2 all-gather.4
  134.8 44.6 all-gather.2
  181.9 151.0 all-reduce.3
  335.4 173.7 reduce-scatter.4
